TPU v7x, 256 devices: a 8x8x2 block of a 8x8x16 slice. The times are simulated.
256 devices in a mesh: grp: 2 (over z), ep: 16 (over y, core), tp: 8 (over x).
Axes of the slice: x: 8, y: 8, z: 2, core: 2. Of those that a mesh axis runs over, the one named last changes fastest.
The devices are a block of a 8x8x16 slice.
Arguments:
- tokens: bfloat16 [12288, 4096], P(('grp', 'ep'), 'tp'), parts along dimension 0
- pre_gain: float32 [4096], replicated, may hold values from 0.1 to 1.9
- out_gain: float32 [4096], P('tp'), may hold values from 0.1 to 1.9
- chosen: int32 [32, 16, 48], P(('grp', 'ep')), parts along dimension 0, may hold values from 0 to 383, as said below
- route_weight: float32 [32, 16, 48], P(('grp', 'ep')), parts along dimension 0, may hold values from 0.3 to 3
- expert_gate: bfloat16 [16, 4096, 3072], P('ep', None, 'tp'), may hold values from -0.09375 to 0.09375
- expert_up: bfloat16 [16, 4096, 3072], P('ep', None, 'tp'), may hold values from -0.09375 to 0.09375
- expert_down: bfloat16 [16, 3072, 4096], P('ep', 'tp'), may hold values from -0.109375 to 0.109375
Outputs:
- output: bfloat16 [12288, 4096], P(('grp', 'ep'), 'tp'), parts along dimension 0
There are 2 independent parts, one for each index of `grp`. A program takes and returns all parts, laid end to end along the dimension named above; an argument that names none is the same for every part. Nothing has to cross between parts.
Inputs may be any that keep to these rules, and one draw needn't show every extreme that they name: chosen[b, e, k] is the position, within block b of 384 tokens, of the k-th token that expert e takes from that block; the 48 positions of one block and one expert are all different.
All inputs are finite; a program needn't handle non-finite values.
Results may differ from a plain program's by a relative error of at most 0.0075.
Values may be sent and summed in bfloat16 or wider, within the bound.
A program may use at most 64 MiB of HBM per device.

v0:
```python
import jax
import jax.numpy as jnp
from jax import lax
from jax.sharding import PartitionSpec as P

NORM_EPS = 1e-06


def sent_to_all(value, axis):
    copies = jnp.broadcast_to(value, (lax.axis_size(axis), *value.shape))
    return lax.all_to_all(copies, axis, split_axis=0, concat_axis=0, tiled=True)


def of_everyone(value, axis):
    return sent_to_all(value, axis).sum(axis=0)


def shards(tokens, pre_gain, out_gain, chosen, route_weight, expert_gate, expert_up, expert_down):
    model_width = pre_gain.shape[0]
    shard_width = tokens.shape[1]
    tok_count = tokens.shape[0]
    chosen_here = chosen[0]
    experts_all = chosen_here.shape[0]
    slot_count = chosen_here.shape[1]
    resident = tokens.astype(jnp.float32)
    square_sum = of_everyone(jnp.sum(resident * resident, axis=1), "tp")
    row_scale = lax.rsqrt(square_sum / model_width + NORM_EPS)[:, None]
    gain_slice = lax.dynamic_slice_in_dim(
        pre_gain, lax.axis_index("tp") * shard_width, shard_width, 0
    )
    normed = (resident * row_scale * gain_slice).astype(jnp.bfloat16)
    outgoing = jnp.take(normed, chosen_here, axis=0)
    incoming = lax.all_to_all(outgoing, "ep", split_axis=0, concat_axis=0, tiled=True)
    picked_rows = lax.all_gather(incoming.reshape(-1, shard_width), "tp", axis=1, tiled=True)
    gate_act = jnp.dot(picked_rows, expert_gate[0], preferred_element_type=jnp.float32)
    up_act = jnp.dot(picked_rows, expert_up[0], preferred_element_type=jnp.float32)
    hidden = (jax.nn.silu(gate_act) * up_act).astype(jnp.bfloat16)
    down_shard = expert_down[0]
    summed = lax.psum_scatter(
        lax.dot_general(
            down_shard, hidden, (((0,), (1,)), ((), ())), preferred_element_type=jnp.float32
        ).astype(jnp.bfloat16),
        "tp",
        scatter_dimension=0,
        tiled=True,
    )
    expert_out = summed.reshape(shard_width, experts_all, slot_count)
    returned = lax.all_to_all(expert_out, "ep", split_axis=1, concat_axis=1, tiled=True)
    weighted = returned.astype(jnp.float32) * route_weight[0][None]
    flat_weighted = weighted.reshape(shard_width, experts_all * slot_count)
    update_cols = (
        jnp.zeros((shard_width, tok_count), jnp.float32)
        .at[:, chosen_here.reshape(-1)]
        .add(flat_weighted)
    )
    mixed_rows = resident + update_cols.T
    out_sum = of_everyone(jnp.sum(mixed_rows * mixed_rows, axis=1), "tp")
    out_scale = lax.rsqrt(out_sum / model_width + NORM_EPS)[:, None]
    return (mixed_rows * out_scale * out_gain).astype(jnp.bfloat16)


def solution(mesh):
    return jax.shard_map(
        shards,
        mesh=mesh,
        in_specs=(
            P(("grp", "ep"), "tp"),
            P(),
            P("tp"),
            P(("grp", "ep"), None, None),
            P(("grp", "ep"), None, None),
            P("ep", None, "tp"),
            P("ep", None, "tp"),
            P("ep", "tp", None),
        ),
        out_specs=P(("grp", "ep"), "tp"),
        check_vma=False,
    )
```

profile of v0, /device:TPU:513, one launch (start us, length us, event | category | flops | bytes accessed | tf_op | source)
XLA Modules:
  0.0 296.7 jit_solution(16021628923282463937)
XLA Ops:
  6.5 0.0 copy-start
  6.6 1.3 fusion.12
  7.9 0.6 broadcast_in_dim.26
  8.5 7.9 %all-to-all-start = ((f32[8,1,384]{2,1,0:T(1,128)}), f32[8,1,384]{2,1,0:T(1,128)S(1)}, u32[]{:S(2)}, u32[]{:S(2)}) async-start(f32[8,1,384]{2,1,0:T(1,128)} %broadcast_in_dim.26), calls=%async_computation | async-start | bytes 24576 | tf_op jit(solution)/shard_map/all_to_all | solution.py:11
  16.3 0.1 all-gather.2.cloned.1.call-start
  16.4 0.7 compare_select_fusion
  17.1 0.7 compare_and_fusion
  17.8 0.1 reshape.96
  17.9 0.8 dynamic_slice.3
  18.6 4.3 %all-to-all-done = f32[8,1,384]{2,1,0:T(1,128)S(1)} async-done(((f32[8,1,384]{2,1,0:T(1,128)}), f32[8,1,384]{2,1,0:T(1,128)S(1)}, u32[]{:S(2)}, u32[]{:S(2)}) %all-to-all-start) | async-done | bytes 12320 | tf_op jit(solution)/shard_map/all_to_all | solution.py:11
  23.0 1.2 fusion.14
  24.1 3.3 %gather_fusion = bf16[768,512]{1,0:T(8,128)(2,1)} fusion(bf16[384,512]{1,0:T(8,128)(2,1)S(1)} %fusion.14, s32[1024]{0:T(1024)S(1)} %pad_clamp_fusion), kind=kCustom, calls=%fused_computation | custom fusion | bytes 1575936 | tf_op jit(solution)/shard_map/jit(_take)/gather | solution.py:32
  27.4 1.3 broadcast_select_fusion
  28.8 43.4 %all_to_all.22 = bf16[16,48,512]{2,1,0:T(8,128)(2,1)} all-to-all(bf16[16,48,512]{2,1,0:T(8,128)(2,1)S(1)} %broadcast_select_fusion), channel_id=1, replica_groups=mesh['grp'=2,'ep'=16,'tp'=8] {'ep'}, dimensions={0} | all-to-all | bytes 1572864 | tf_op jit(solution)/shard_map/all_to_all | solution.py:33
  72.1 0.1 all-gather.2.cloned.1.call-update
  72.2 0.1 reduce-scatter.2.cloned.1.call-start
  72.3 71.5 %all-gather.2.cloned.1.call-done = bf16[768,4096]{1,0:T(8,128)(2,1)} async-done(((bf16[768,512]{1,0:T(8,128)(2,1)}), bf16[768,4096]{1,0:T(8,128)(2,1)}) %all-gather.2.cloned.1.call-update) | async-done | bytes 6291472 | tf_op jit(solution)/shard_map/all_gather | solution.py:34
  143.8 0.0 copy-start.3
  143.8 0.0 copy-start.4
  143.8 6.6 %fusion.4 = f32[768,384]{1,0:T(8,128)S(1)} fusion(bf16[768,4096]{1,0:T(8,128)(2,1)} %all-gather.2.cloned.1.call-done, bf16[1,4096,384]{2,1,0:T(8,128)(2,1)} %param.13), kind=kOutput, calls=%fused_computation.7 | convolution fusion | flops 2415919104 | bytes 10616832 | tf_op jit(solution)/shard_map/dot_general | solution.py:35
  150.4 0.0 copy-done.3
  150.4 0.0 copy-done.4
  150.4 3.5 %fusion.9 = bf16[768,384]{1,0:T(8,128)(2,1)S(1)} fusion(bf16[768,4096]{1,0:T(8,128)(2,1)S(1)} %copy-done.3, bf16[1,4096,384]{2,1,0:T(8,128)(2,1)S(1)} %copy-done.4, f32[768,384]{1,0:T(8,128)S(1)} %fusion.4), kind=kOutput, calls=%fused_computation.11 | convolution fusion | flops 2417688576 | bytes 11206656 | tf_op jit(solution)/shard_map/dot_general | solution.py:36
  153.9 0.0 copy-done
  153.9 5.3 %fusion = bf16[4096,768]{0,1:T(8,128)(2,1)} fusion(bf16[768,384]{1,0:T(8,128)(2,1)S(1)} %fusion.9, bf16[1,384,4096]{2,1,0:T(8,128)(2,1)S(1)} %copy-done), kind=kOutput, calls=%fused_computation.3 | convolution fusion | flops 2419064832 | bytes 10027008 | tf_op jit(solution)/shard_map/dot_general | solution.py:40
  159.2 0.0 copy-start.2
  159.2 0.1 reduce-scatter.2.cloned.1.call-update
  159.2 0.0 copy-start.1
  159.3 75.4 %reduce-scatter.2.cloned.1.call-done = bf16[512,768]{0,1:T(8,128)(2,1)} async-done(((bf16[4096,768]{0,1:T(8,128)(2,1)}), bf16[512,768]{0,1:T(8,128)(2,1)}) %reduce-scatter.2.cloned.1.call-update) | async-done | bytes 786448 | tf_op jit(solution)/shard_map/reduce_scatter | solution.py:39
  234.7 7.7 %all-to-all-start.2 = ((bf16[512,16,48]{0,2,1:T(8,128)(2,1)}), bf16[512,16,48]{0,2,1:T(8,128)(2,1)}, u32[]{:S(2)}, u32[]{:S(2)}) async-start(bf16[512,16,48]{0,2,1:T(8,128)(2,1)} %bitcast.42), calls=%async_computation.3 | async-start | bytes 1572864 | tf_op jit(solution)/shard_map/all_to_all | solution.py:48
  242.4 0.0 copy-done.2
  242.4 0.1 reshape_squeeze.3
  242.5 22.7 %all-to-all-done.2 = bf16[512,16,48]{0,2,1:T(8,128)(2,1)} async-done(((bf16[512,16,48]{0,2,1:T(8,128)(2,1)}), bf16[512,16,48]{0,2,1:T(8,128)(2,1)}, u32[]{:S(2)}, u32[]{:S(2)}) %all-to-all-start.2) | async-done | bytes 786464 | tf_op jit(solution)/shard_map/all_to_all | solution.py:48
  265.2 2.5 convert_multiply_fusion
  267.7 8.1 %scatter_custom_fusion = f32[512,384]{0,1:T(8,128)} fusion(s32[768]{0:T(1024)S(1)} %fusion.17, f32[768,512]{1,0:T(8,128)} %bitcast.41, f32[]{:T(128)} %constant.11.clone.1), kind=kCustom, calls=%fused_computation.21 | custom fusion | flops 393216 | bytes 786944 | tf_op jit(solution)/shard_map/scatter-add | solution.py:54
  275.8 0.0 copy-done.1
  275.9 1.3 multiply_reduce_fusion
  277.2 10.7 %all_to_all.23 = f32[8,1,384]{2,1,0:T(1,128)S(1)} all-to-all(f32[8,1,384]{2,1,0:T(1,128)S(1)} %broadcast_in_dim.28), channel_id=1, replica_groups=mesh['grp'=2,'ep'=16,'tp'=8] {'tp'}, dimensions={0} | all-to-all | bytes 24576 | tf_op jit(solution)/shard_map/all_to_all | solution.py:11
  287.9 2.0 multiply_convert_fusion
  (7 shorter events, 0.1 us)
Async XLA Ops:
  6.5 147.3 %copy-start = (bf16[1,384,4096]{2,1,0:T(8,128)(2,1)S(1)}, bf16[1,384,4096]{2,1,0:T(8,128)(2,1)}, u32[]{:S(2)}) copy-start(bf16[1,384,4096]{2,1,0:T(8,128)(2,1)} %param.15) | copy-start | bytes 9437188
  8.5 14.5 %all-to-all-start = ((f32[8,1,384]{2,1,0:T(1,128)}), f32[8,1,384]{2,1,0:T(1,128)S(1)}, u32[]{:S(2)}, u32[]{:S(2)}) async-start(f32[8,1,384]{2,1,0:T(1,128)} %broadcast_in_dim.26), calls=%async_computation | async-start | bytes 24576 | tf_op jit(solution)/shard_map/all_to_all | solution.py:11
  16.3 127.5 %all-gather.2.cloned.1.call-start = ((), (), s32[]{:S(2)}) async-start(), calls=%async_computation.5 | async-start | bytes 7077888 | tf_op jit(solution)/shard_map/all_gather | solution.py:34
  72.2 162.5 %reduce-scatter.2.cloned.1.call-start = ((), (), s32[]{:S(2)}) async-start(), calls=%async_computation.6 | async-start | bytes 7077888 | tf_op jit(solution)/shard_map/reduce_scatter | solution.py:39
  143.8 6.6 %copy-start.3 = (bf16[768,4096]{1,0:T(8,128)(2,1)S(1)}, bf16[768,4096]{1,0:T(8,128)(2,1)}, u32[]{:S(2)}) copy-start(bf16[768,4096]{1,0:T(8,128)(2,1)} %all-gather.2.cloned.1.call-done) | copy-start | bytes 18874372
  143.8 6.6 %copy-start.4 = (bf16[1,4096,384]{2,1,0:T(8,128)(2,1)S(1)}, bf16[1,4096,384]{2,1,0:T(8,128)(2,1)}, u32[]{:S(2)}) copy-start(bf16[1,4096,384]{2,1,0:T(8,128)(2,1)} %param.14) | copy-start | bytes 9437188
  159.2 83.2 %copy-start.2 = (s32[1,16,48]{2,1,0:T(8,128)S(1)}, s32[1,16,48]{2,1,0:T(8,128)}, u32[]{:S(2)}) copy-start(s32[1,16,48]{2,1,0:T(8,128)} %param.11) | copy-start | bytes 9220
  159.2 116.6 %copy-start.1 = (bf16[384,512]{1,0:T(8,128)(2,1)S(1)}, bf16[384,512]{1,0:T(8,128)(2,1)}, u32[]{:S(2)}) copy-start(bf16[384,512]{1,0:T(8,128)(2,1)} %param.8) | copy-start | bytes 1179652
  234.7 30.6 %all-to-all-start.2 = ((bf16[512,16,48]{0,2,1:T(8,128)(2,1)}), bf16[512,16,48]{0,2,1:T(8,128)(2,1)}, u32[]{:S(2)}, u32[]{:S(2)}) async-start(bf16[512,16,48]{0,2,1:T(8,128)(2,1)} %bitcast.42), calls=%async_computation.3 | async-start | bytes 1572864 | tf_op jit(solution)/shard_map/all_to_all | solution.py:48
Sparse Core Ops, SparseCore 0:
  72.3 71.4 all-gather.1
  159.4 75.2 reduce-scatter.1
where the time goes:
time: 297 us
  waiting for transfers between devices  174 us (59%)
  blocking collectives  54 us (18%)
  other arithmetic  19.2 us (6%)
  starting transfers between devices  15.7 us (5%)
  matrix products  15.4 us (5%)
  between operations  13.5 us (5%)
  local copies, waits for them, and re-layouts  4.88 us (2%)
    reduce_scatter x1, waiting for transfers between devices, shards(): lax.psum_scatter(lax.dot_general(down_shard, hidden, (((0,), (1,)), ((),...  75.4 us
    all_gather x1, waiting for transfers between devices, shards(): lax.all_gather(incoming.reshape(-1, shard_width), 'tp', axis=1, tiled=True)  71.5 us
    all_to_all x1, blocking collectives, shards(): lax.all_to_all(outgoing, 'ep', split_axis=0, concat_axis=0, tiled=True)  43.4 us
    all_to_all x1, waiting for transfers between devices, shards(): lax.all_to_all(expert_out, 'ep', split_axis=1, concat_axis=1, tiled=True)  22.7 us
    all_to_all x1, blocking collectives, sent_to_all(): return lax.all_to_all(copies, axis, split_axis=0, concat_axis=0, tiled=True)  10.7 us
    scatter-add x1, other arithmetic, shards(): update_cols = jnp.zeros((shard_width, tok_count), jnp.float32).at[:, chos...  8.14 us
    all_to_all x1, starting transfers between devices, sent_to_all(): return lax.all_to_all(copies, axis, split_axis=0, concat_axis=0, tiled=True)  7.86 us
    all_to_all x1, starting transfers between devices, shards(): lax.all_to_all(expert_out, 'ep', split_axis=1, concat_axis=1, tiled=True)  7.72 us
  transfers between devices with their start and end apart: 4, of which 4 were waited for; matrix products, arithmetic and copies ran while one was open for 1% of the time, Pallas kernels for 0%

commit v1 on v0

v1 whole, which is shorter than its diff:
```python
import functools

import jax
import jax.numpy as jnp
from jax import lax
from jax.experimental import pallas as pl
from jax.experimental.pallas import tpu as pltpu
from jax.sharding import PartitionSpec as P

NORM_EPS = 1e-06
MESH = pl.DeviceIdType.MESH
RIGHT, LEFT = 0, 1
EVEN, ODD = 0, 1

SLOTS = {
    8: (7, {(RIGHT, EVEN): (0, 3, 6, 9), (RIGHT, ODD): (5, 8, 11),
            (LEFT, EVEN): (0, 3, 6), (LEFT, ODD): (2, 5, 8, 11)}),
    4: (3, {(RIGHT, EVEN): (0, 4), (RIGHT, ODD): (2,),
            (LEFT, EVEN): (0,), (LEFT, ODD): (1, 5)}),
}


def kernel(n_ep, n_tp, tokens, pre_gain, out_gain, chosen, route, w_gate, w_up, w_down,
           out,
           picks, gathered, normed, w_gu, w_dn, gate_up, hidden, partial, chain, summed,
           returned, mix_hi, mix_lo, mixed, squares,
           load_sem, disp_s, disp_r, ag_s, ag_r, rs_s, rs_r, ret_s, ret_r, sq_s, sq_r):
    bf16, f32 = jnp.bfloat16, jnp.float32
    tok, width = tokens.shape
    slots = chosen.shape[1]
    ffw = w_down.shape[0]
    chunk = 2 * slots
    n_y = n_ep // 2
    n_pair = n_y // 2
    rs0 = max(n_pair, 4)
    period, table = SLOTS[n_tp]
    model_width = n_tp * width

    ep = lax.axis_index("ep")
    tp = lax.axis_index("tp")
    y = ep // 2

    def wrap(v, n):
        return lax.rem(v + 2 * n, n)

    def rows(at, size):
        return pl.ds(pl.multiple_of(at * size, size), size)

    right, left = wrap(tp + 1, n_tp), wrap(tp - 1, n_tp)

    loads = [
        pltpu.make_async_copy(w_gate, w_gu.at[:, pl.ds(0, ffw)], load_sem.at[0]),
        pltpu.make_async_copy(w_up, w_gu.at[:, pl.ds(ffw, ffw)], load_sem.at[1]),
        pltpu.make_async_copy(w_down, w_dn, load_sem.at[2]),
    ]
    for load in loads:
        load.start()

    barrier = pltpu.get_barrier_semaphore()
    for k in range(1, n_ep):
        pl.semaphore_signal(barrier, inc=1, device_id={"ep": wrap(ep + k, n_ep)}, device_id_type=MESH)
    for k in range(1, n_tp):
        pl.semaphore_signal(barrier, inc=1, device_id={"tp": wrap(tp + k, n_tp)}, device_id_type=MESH)

    chosen_t = jnp.transpose(chosen[...].astype(f32))
    lane = lax.broadcasted_iota(jnp.int32, (slots, tok), 1).astype(f32)
    for e in range(n_ep):
        hot = jnp.where(chosen_t[:, e:e + 1] == lane, 1.0, 0.0).astype(bf16)
        picks[e * slots:(e + 1) * slots, :] = jnp.dot(
            hot, tokens[...], preferred_element_type=f32).astype(bf16)
    gathered[tp, rows(ep, slots), :] = picks[rows(ep, slots), :]

    pl.semaphore_wait(barrier, n_ep - 1 + n_tp - 1)

    def dispatch(e):
        return pltpu.make_async_remote_copy(
            src_ref=picks.at[rows(e, slots), :],
            dst_ref=gathered.at[tp, rows(ep, slots), :],
            send_sem=disp_s.at[e], recv_sem=disp_r.at[ep],
            device_id={"ep": e}, device_id_type=MESH)

    def dispatched(b):
        return pltpu.make_async_remote_copy(
            src_ref=picks.at[rows(b, slots), :],
            dst_ref=gathered.at[tp, rows(b, slots), :],
            send_sem=disp_s.at[b], recv_sem=disp_r.at[b],
            device_id={"ep": b}, device_id_type=MESH)

    dispatch(ep + 1 - 2 * lax.rem(ep, 2)).start()
    for j in range(n_pair):
        for rel in ((j, -j - 1) if j else (-1,)):
            for core in range(2):
                dispatch(2 * wrap(y + rel, n_y) + core).start()

    for row in range(0, tok, 128):
        mixed[row:row + 128, :] = tokens[row:row + 128, :].astype(f32)

    def chip_in(pair, par):
        return wrap(y - pair, n_y) if par == EVEN else wrap(y + pair + 1, n_y)

    def chip_back(step, par):
        pair = lax.rem(step + 1, n_pair)
        return wrap(y + pair + 1, n_y) if par == EVEN else wrap(y - pair, n_y)

    def ag(d, c, h):
        sign = 1 if d == RIGHT else -1
        at = (wrap(tp - sign * (h - 1), n_tp), rows(c, chunk), slice(None))
        return pltpu.make_async_remote_copy(
            src_ref=gathered.at[at], dst_ref=gathered.at[at],
            send_sem=ag_s.at[d, c, h - 1], recv_sem=ag_r.at[d, c, h - 1],
            device_id={"tp": right if d == RIGHT else left}, device_id_type=MESH)

    def ag_in(d, c, h):
        sign = 1 if d == RIGHT else -1
        at = (wrap(tp - sign * h, n_tp), rows(c, chunk), slice(None))
        return pltpu.make_async_remote_copy(
            src_ref=gathered.at[at], dst_ref=gathered.at[at],
            send_sem=ag_s.at[d, c, h - 1], recv_sem=ag_r.at[d, c, h - 1],
            device_id={"tp": left if d == RIGHT else right}, device_id_type=MESH)

    def rs(d, c, h, dest):
        src = partial.at[dest, rows(c, chunk), :] if h == 1 else chain.at[d, c, h - 2]
        return pltpu.make_async_remote_copy(
            src_ref=src, dst_ref=chain.at[d, c, h - 1],
            send_sem=rs_s.at[d, c, h - 1], recv_sem=rs_r.at[d, c, h - 1],
            device_id={"tp": right if d == RIGHT else left}, device_id_type=MESH)

    def wait_dispatched(c):
        for core in range(2):
            b = 2 * c + core

            @pl.when(b != ep)
            def _():
                dispatched(b).wait_recv()

    def send_gather(d, par, h, pair):
        c = chip_in(pair, par)
        if h > 1:
            ag_in(d, c, h - 1).wait_recv()
        ag(d, c, h).start()

    def send_reduce(d, par, h, step):
        hops = len(table[d, par])
        c = chip_back(step, par)
        sign = 1 if d == RIGHT else -1
        dest = wrap(tp + sign * (hops - h + 1), n_tp)
        if h > 1:
            rs(d, c, h - 1, dest).wait_recv()
            mine = partial[dest, rows(c, chunk), :].astype(f32)
            chain[d, c, h - 2] = (chain[d, c, h - 2].astype(f32) + mine).astype(bf16)
        rs(d, c, h, dest).start()

    def norm_pair(pair):
        for par in (EVEN, ODD):
            c = chip_in(pair, par)
            for d in (RIGHT, LEFT):
                ag_in(d, c, len(table[d, par])).wait_recv()
            total = jnp.zeros((chunk, 128), f32)
            for t in range(n_tp):
                for k in range(0, width, 128):
                    v = gathered[t, rows(c, chunk), k:k + 128].astype(f32)
                    total = total + v * v
            mean = jnp.sum(total, axis=1, keepdims=True) / model_width
            scale = lax.rsqrt(mean + NORM_EPS)
            for t in range(n_tp):
                v = gathered[t, rows(c, chunk), :].astype(f32)
                g = pre_gain[:, t * width:(t + 1) * width]
                normed[par * chunk:(par + 1) * chunk, t * width:(t + 1) * width] = (
                    v * scale * g).astype(bf16)

    gu_tile = 2 * ffw // 3 if (2 * ffw // 3) % 128 == 0 else 2 * ffw

    def gate_up_tile(n):
        at = slice(n * gu_tile, (n + 1) * gu_tile)
        gate_up[:, at] = jnp.dot(normed[...], w_gu[:, at], preferred_element_type=f32)

    def activate():
        g = gate_up[:, :ffw]
        u = gate_up[:, ffw:]
        hidden[...] = (g / (1.0 + jnp.exp(-g)) * u).astype(bf16)

    def down_tile(pair, t):
        res = jnp.dot(hidden[...], w_dn[:, t * width:(t + 1) * width],
                      preferred_element_type=f32).astype(bf16)
        partial[t, rows(chip_in(pair, EVEN), chunk), :] = res[:chunk]
        partial[t, rows(chip_in(pair, ODD), chunk), :] = res[chunk:]

    def mix_matrix(c):
        e = 2 * c
        picked = jnp.concatenate([chosen[pl.ds(e, 1), :], chosen[pl.ds(e + 1, 1), :]], axis=1)
        weight = jnp.concatenate([route[pl.ds(e, 1), :], route[pl.ds(e + 1, 1), :]], axis=1)
        for row in range(0, tok, 128):
            at = lax.broadcasted_iota(jnp.int32, (128, chunk), 0) + row
            w = jnp.where(at == picked, weight, 0.0)
            hi = w.astype(bf16)
            mix_hi[c, row:row + 128, :] = hi
            mix_lo[c, row:row + 128, :] = (w - hi.astype(f32)).astype(bf16)

    def give_back(e_block):
        return pltpu.make_async_remote_copy(
            src_ref=summed.at[rows(e_block, slots), :],
            dst_ref=returned.at[rows(ep, slots), :],
            send_sem=ret_s.at[e_block], recv_sem=ret_r.at[ep],
            device_id={"ep": e_block}, device_id_type=MESH)

    def given_back(e):
        return pltpu.make_async_remote_copy(
            src_ref=summed.at[rows(e, slots), :],
            dst_ref=returned.at[rows(e, slots), :],
            send_sem=ret_s.at[e], recv_sem=ret_r.at[e],
            device_id={"ep": e}, device_id_type=MESH)

    def finish_chunk(step, par):
        c = chip_back(step, par)
        total = partial[tp, rows(c, chunk), :].astype(f32)
        for d in (RIGHT, LEFT):
            hops = len(table[d, par])
            rs(d, c, hops, tp).wait_recv()
            total = total + chain[d, c, hops - 1].astype(f32)
        summed[rows(c, chunk), :] = total.astype(bf16)
        for core in range(2):
            b = 2 * c + core

            @pl.when(b != ep)
            def _():
                give_back(b).start()

            @pl.when(b == ep)
            def _():
                returned[rows(b, slots), :] = summed[rows(b, slots), :]

    def combine(step):
        pair = lax.rem(step + 1, n_pair)
        for c in (wrap(y - pair - 1, n_y), wrap(y + pair, n_y)):
            for core in range(2):
                e = 2 * c + core

                @pl.when(e != ep)
                def _():
                    given_back(e).wait_recv()
            rhs = returned[rows(c, chunk), :]
            mixed[...] += (jnp.dot(mix_hi[c], rhs, preferred_element_type=f32)
                           + jnp.dot(mix_lo[c], rhs, preferred_element_type=f32))

    n_gu = 2 * ffw // gu_tile
    pieces = [("norm",)] + [("gu", n) for n in range(n_gu)] + [("act",)] + [("dn", t) for t in range(n_tp)]
    share = -(-len(pieces) // (period - 1))

    def run_piece(piece, pair):
        if piece[0] == "norm":
            norm_pair(pair)
        elif piece[0] == "gu":
            gate_up_tile(piece[1])
        elif piece[0] == "act":
            activate()
        else:
            down_tile(pair, piece[1])

    last = rs0 + n_pair

    def round_(i, carry):
        @pl.when(i == 1)
        def _():
            for load in loads:
                load.wait()

        for k in range(period):
            for par, first in ((EVEN, 0), (ODD, min(table[RIGHT, ODD][0], table[LEFT, ODD][0]))):
                if first == k:
                    @pl.when(i < n_pair)
                    def _():
                        wait_dispatched(chip_in(i, par))
            for (d, par), offsets in table.items():
                for h, at in enumerate(offsets, 1):
                    if at % period != k:
                        continue
                    ii = i - at // period

                    @pl.when((ii >= 0) & (ii < n_pair))
                    def _():
                        send_gather(d, par, h, ii)

                    @pl.when((ii >= rs0) & (ii < rs0 + n_pair))
                    def _():
                        send_reduce(d, par, h, ii - rs0)

            pair = i - 2
            if k < period - 1:
                @pl.when((pair >= 0) & (pair < n_pair))
                def _():
                    for piece in pieces[k * share:(k + 1) * share]:
                        run_piece(piece, pair)

                if k == 0:
                    @pl.when(i < n_pair)
                    def _():
                        for par in (EVEN, ODD):
                            mix_matrix(chip_in(i, par))
        done = i - rs0 - 1

        @pl.when((done >= 0) & (done < n_pair))
        def _():
            for par in (EVEN, ODD):
                finish_chunk(done, par)

        @pl.when((done >= 1) & (done < n_pair))
        def _():
            combine(done - 1)
        return carry

    lax.fori_loop(0, last + 1, round_, 0)
    combine(n_pair - 1)

    part = jnp.zeros((tok, 128), f32)
    for k in range(0, width, 128):
        v = mixed[:, k:k + 128]
        part = part + v * v
    row_sum = lax.dot_general(jnp.ones((8, 128), f32), part, (((1,), (1,)), ((), ())),
                              precision=lax.Precision.HIGHEST, preferred_element_type=f32)
    squares[tp] = row_sum[0:1, :]

    def share_squares(peer):
        return pltpu.make_async_remote_copy(
            src_ref=squares.at[tp], dst_ref=squares.at[tp],
            send_sem=sq_s.at[peer], recv_sem=sq_r.at[tp],
            device_id={"tp": peer}, device_id_type=MESH)

    def shared_squares(peer):
        return pltpu.make_async_remote_copy(
            src_ref=squares.at[peer], dst_ref=squares.at[peer],
            send_sem=sq_s.at[peer], recv_sem=sq_r.at[peer],
            device_id={"tp": peer}, device_id_type=MESH)

    for k in range(1, n_tp):
        share_squares(wrap(tp + k, n_tp)).start()

    def sent_pair(pair, carry):
        for (d, par), offsets in table.items():
            for h in range(1, len(offsets) + 1):
                ag(d, chip_in(pair, par), h).wait_send()
                rs(d, chip_back(pair, par), h, tp).wait_send()
        return carry

    lax.fori_loop(0, n_pair, sent_pair, 0)

    def sent_block(k, carry):
        b = wrap(ep + k, n_ep)
        dispatch(b).wait_send()
        give_back(b).wait_send()
        return carry

    lax.fori_loop(1, n_ep, sent_block, 0)

    for k in range(1, n_tp):
        shared_squares(wrap(tp + k, n_tp)).wait_recv()
    total = squares[0]
    for t in range(1, n_tp):
        total = total + squares[t]
    scale_row = lax.rsqrt(total / model_width + NORM_EPS)
    scale = jnp.transpose(jnp.broadcast_to(scale_row, (8, tok)))[:, 0:1]
    out[...] = (mixed[...] * scale * out_gain[...]).astype(bf16)
    for k in range(1, n_tp):
        share_squares(wrap(tp + k, n_tp)).wait_send()


def solution(mesh):
    n_ep, n_tp = mesh.shape["ep"], mesh.shape["tp"]

    def shards(tokens, pre_gain, out_gain, chosen, route_weight, expert_gate, expert_up, expert_down):
        tok, width = tokens.shape
        slots = chosen.shape[2]
        ffw = expert_gate.shape[2]
        model_width = pre_gain.shape[0]
        cap = n_ep * slots
        chunk = 2 * slots
        n_y = n_ep // 2
        hops = n_tp // 2
        bf16, f32 = jnp.bfloat16, jnp.float32
        vmem = pl.BlockSpec(memory_space=pltpu.VMEM)
        hbm = pl.BlockSpec(memory_space=pl.ANY)
        dma = pltpu.SemaphoreType.DMA
        return pl.pallas_call(
            functools.partial(kernel, n_ep, n_tp),
            name="routed_ffn",
            out_shape=jax.ShapeDtypeStruct((tok, width), bf16),
            in_specs=[vmem] * 5 + [hbm] * 3,
            out_specs=vmem,
            scratch_shapes=[
                pltpu.VMEM((cap, width), bf16),
                pltpu.VMEM((n_tp, cap, width), bf16),
                pltpu.VMEM((2 * chunk, model_width), bf16),
                pltpu.VMEM((model_width, 2 * ffw), bf16),
                pltpu.VMEM((ffw, model_width), bf16),
                pltpu.VMEM((2 * chunk, 2 * ffw), f32),
                pltpu.VMEM((2 * chunk, ffw), bf16),
                pltpu.VMEM((n_tp, cap, width), bf16),
                pltpu.VMEM((2, n_y, hops, chunk, width), bf16),
                pltpu.VMEM((cap, width), bf16),
                pltpu.VMEM((cap, width), bf16),
                pltpu.VMEM((n_y, tok, chunk), bf16),
                pltpu.VMEM((n_y, tok, chunk), bf16),
                pltpu.VMEM((tok, width), f32),
                pltpu.VMEM((n_tp, 1, tok), f32),
                dma((3,)),
                dma((n_ep,)), dma((n_ep,)),
                dma((2, n_y, hops)), dma((2, n_y, hops)),
                dma((2, n_y, hops)), dma((2, n_y, hops)),
                dma((n_ep,)), dma((n_ep,)),
                dma((n_tp,)), dma((n_tp,)),
            ],
            compiler_params=pltpu.CompilerParams(
                collective_id=0, has_side_effects=True, vmem_limit_bytes=60 * 2**20),
        )(tokens, pre_gain.reshape(1, -1), out_gain.reshape(1, -1), chosen[0], route_weight[0],
          expert_gate[0], expert_up[0], expert_down[0])

    return jax.shard_map(
        shards,
        mesh=mesh,
        in_specs=(
            P(("grp", "ep"), "tp"),
            P(),
            P("tp"),
            P(("grp", "ep"), None, None),
            P(("grp", "ep"), None, None),
            P("ep", None, "tp"),
            P("ep", None, "tp"),
            P("ep", "tp", None),
        ),
        out_specs=P(("grp", "ep"), "tp"),
        check_vma=False,
    )
```

time: 297 us -> 165 us (0.56)
  waiting for transfers between devices: 174 us -> 0 us
  Pallas kernels: 0 us -> 163 us
  blocking collectives: 54 us -> 0 us
  other arithmetic: 19.2 us -> 0 us
  starting transfers between devices: 15.7 us -> 0 us
  matrix products: 15.4 us -> 0 us
  between operations: 13.5 us -> 0.01 us
  local copies, waits for them, and re-layouts: 4.88 us -> 1.77 us
    pallas_call x0 -> x1, Pallas kernels: none -> 163 us  [shards(): pl.pallas_call(functools.partial(kernel, n_ep, n_tp), name='routed_ffn',...]
    reduce_scatter x1 -> x0, waiting for transfers between devices: 75.4 us -> none  [shards(): lax.psum_scatter(lax.dot_general(down_shard, hidden, (((0,), (1,)), ((),...]
    all_gather x1 -> x0, waiting for transfers between devices: 71.5 us -> none  [shards(): lax.all_gather(incoming.reshape(-1, shard_width), 'tp', axis=1, tiled=True)]
    all_to_all x2 -> x0, blocking collectives: 54 us -> none  [the longest x1 43.4 us: shards(): lax.all_to_all(outgoing, 'ep', split_axis=0, concat_axis=0, tiled=True)]
    all_to_all x2 -> x0, waiting for transfers between devices: 27 us -> none  [the longest x1 22.7 us: shards(): lax.all_to_all(expert_out, 'ep', split_axis=1, concat_axis=1, tiled=True)]
    all_to_all x2 -> x0, starting transfers between devices: 15.6 us -> none  [the longest x1 7.86 us: sent_to_all(): return lax.all_to_all(copies, axis, split_axis=0, concat_axis=0, tiled=True)]
    dot_general x3 -> x0, matrix products: 15.4 us -> none  [the longest x1 6.57 us: shards(): jnp.dot(picked_rows, expert_gate[0], preferred_element_type=jnp.float32)]
    scatter-add x1 -> x0, other arithmetic: 8.14 us -> none  [shards(): update_cols = jnp.zeros((shard_width, tok_count), jnp.float32).at[:, chos...]
  transfers between devices with their start and end apart: 4 -> 0, of which waited for: 4 -> 0; matrix products, arithmetic and copies ran while one was open for 1% -> 0% of each run, Pallas kernels for 0% -> 0%
where the time goes in v1:
time: 165 us
  Pallas kernels  163 us (99%)
  local copies, waits for them, and re-layouts  1.77 us (1%)
    pallas_call x1, Pallas kernels, shards(): pl.pallas_call(functools.partial(kernel, n_ep, n_tp), name='routed_ffn',...  163 us

profile of v1, /device:TPU:513, one launch (start us, length us, event | category | flops | bytes accessed | tf_op | source)
XLA Modules:
  0.0 164.5 jit_solution(8905548700569053716)
XLA Ops:
  0.0 162.7 %routed_ffn.1 = bf16[384,512]{1,0:T(8,128)(2,1)} custom-call(bf16[384,512]{1,0:T(8,128)(2,1)} %tokens.1, f32[1,4096]{1,0:T(1,128)} %bitcast.10, f32[1,512]{1,0:T(1,128)} %bitcast.13, s32[16,48]{1,0:T(8,128)} %bitcast.11, f32[16,48]{1,0:T(8,128)} %bitcast.12, bf16[4096,384]{1,0:T(8,128)(2,1)} %bitcast.7, bf16[4096,384]{1,0:T(8,128)(2,1)} %bitcast.8, ...), custom_call_target="tpu_custom_call" | custom-call | tf_op jit(solution)/shard_map/routed_ffn/pallas_call | solution.py:382
  162.7 1.8 %copy.10 = bf16[384,512]{1,0:T(8,128)(2,1)} copy(bf16[384,512]{1,0:T(8,128)(2,1)} %routed_ffn.1) | data formatting | bytes 786432

commit v2 on v1

v2 whole, which is shorter than its diff:
```python
import functools

import jax
import jax.numpy as jnp
from jax import lax
from jax.experimental import pallas as pl
from jax.experimental.pallas import tpu as pltpu
from jax.sharding import PartitionSpec as P

NORM_EPS = 1e-06
MESH = pl.DeviceIdType.MESH
RIGHT, LEFT = 0, 1
EVEN, ODD = 0, 1

SLOTS = {
    8: (7, {(RIGHT, EVEN): (0, 3, 6, 9), (RIGHT, ODD): (5, 8, 11),
            (LEFT, EVEN): (0, 3, 6), (LEFT, ODD): (2, 5, 8, 11)}),
    4: (3, {(RIGHT, EVEN): (0, 4), (RIGHT, ODD): (2,),
            (LEFT, EVEN): (0,), (LEFT, ODD): (1, 5)}),
}


def kernel(n_ep, n_tp, tokens_in, pre_gain_in, chosen_in, route_in, w_gate, w_up, w_down,
           mixed, scale_out,
           tokens, pre_gain, chosen, route, hot, picks, gathered, normed, w_gu, w_dn, gate_up, hidden,
           partial, chain, summed, returned, mix, squares,
           load_sem, disp_s, disp_r, ag_s, ag_r, rs_s, rs_r, ret_s, ret_r, sq_s, sq_r):
    bf16, f32 = jnp.bfloat16, jnp.float32
    tok, width = tokens.shape
    slots = chosen.shape[1]
    ffw = w_down.shape[0]
    chunk = 2 * slots
    n_y = n_ep // 2
    n_pair = n_y // 2
    rs0 = max(n_pair, 4)
    period, table = SLOTS[n_tp]
    model_width = n_tp * width

    ep = lax.axis_index("ep")
    tp = lax.axis_index("tp")
    y = ep // 2
    core = lax.rem(ep, 2)

    def wrap(v, n):
        return lax.rem(v + 2 * n, n)

    def rows(at, size):
        return pl.ds(pl.multiple_of(at * size, size), size)

    right, left = wrap(tp + 1, n_tp), wrap(tp - 1, n_tp)

    barrier = pltpu.get_barrier_semaphore()
    for k in range(1, n_ep):
        pl.semaphore_signal(barrier, inc=1, device_id={"ep": wrap(ep + k, n_ep)}, device_id_type=MESH)
    for k in range(1, n_tp):
        pl.semaphore_signal(barrier, inc=1, device_id={"tp": wrap(tp + k, n_tp)}, device_id_type=MESH)

    early = [pltpu.make_async_copy(src, dst, load_sem.at[k])
             for k, (src, dst) in enumerate(((chosen_in, chosen), (tokens_in, tokens)))]
    late = [pltpu.make_async_copy(src, dst, load_sem.at[k + 2])
            for k, (src, dst) in enumerate((
                (route_in, route), (pre_gain_in, pre_gain), (w_gate, w_gu.at[:, pl.ds(0, ffw)]),
                (w_up, w_gu.at[:, pl.ds(ffw, ffw)]), (w_down, w_dn)))]
    for load in early + late:
        load.start()

    early[0].wait()
    chosen_t = jnp.transpose(chosen[...].astype(f32))
    lane = lax.broadcasted_iota(jnp.int32, (slots, tok), 1).astype(f32)
    for e in range(n_ep):
        hot[e * slots:(e + 1) * slots, :] = jnp.where(chosen_t[:, e:e + 1] == lane, 1.0, 0.0).astype(bf16)
    early[1].wait()
    part_rows = n_ep * slots // 4
    for k in range(4):
        at = slice(k * part_rows, (k + 1) * part_rows)
        picks[at, :] = jnp.dot(hot[at, :], tokens[...], preferred_element_type=f32).astype(bf16)
    gathered[tp, rows(ep, slots), :] = picks[rows(ep, slots), :]

    pl.semaphore_wait(barrier, n_ep - 1 + n_tp - 1)

    def dispatch(e, to):
        return pltpu.make_async_remote_copy(
            src_ref=picks.at[rows(e, slots), :],
            dst_ref=gathered.at[tp, rows(to, slots), :],
            send_sem=disp_s.at[e], recv_sem=disp_r.at[to],
            device_id={"ep": e}, device_id_type=MESH)

    def chip_in(pair, par):
        return wrap(y - pair, n_y) if par == EVEN else wrap(y + pair + 1, n_y)

    def chip_back(step, par):
        pair = lax.rem(step + 1, n_pair)
        return wrap(y + pair + 1, n_y) if par == EVEN else wrap(y - pair, n_y)

    def blocks_in(c):
        return 2 * c + core, 2 * c + 1 - core

    def blocks_back(c):
        return 2 * c + 1 - core, 2 * c + core

    def ag(d, b, h, slice_at):
        sign = 1 if d == RIGHT else -1
        at = (wrap(tp - sign * slice_at, n_tp), rows(b, slots), slice(None))
        return pltpu.make_async_remote_copy(
            src_ref=gathered.at[at], dst_ref=gathered.at[at],
            send_sem=ag_s.at[d, b, h - 1], recv_sem=ag_r.at[d, b, h - 1],
            device_id={"tp": right if d == RIGHT else left}, device_id_type=MESH)

    def rs(d, b, h, dest):
        src = partial.at[dest, rows(b, slots), :] if h == 1 else chain.at[d, b, h - 2]
        return pltpu.make_async_remote_copy(
            src_ref=src, dst_ref=chain.at[d, b, h - 1],
            send_sem=rs_s.at[d, b, h - 1], recv_sem=rs_r.at[d, b, h - 1],
            device_id={"tp": right if d == RIGHT else left}, device_id_type=MESH)

    def wait_dispatched(b):
        @pl.when(b != ep)
        def _():
            dispatch(b, b).wait_recv()

    def gather_block(d, b, h):
        if h > 1:
            ag(d, b, h - 1, h - 1).wait_recv()
        ag(d, b, h, h - 1).start()

    def send_gather(d, par, h, pair):
        for b in blocks_in(chip_in(pair, par)):
            gather_block(d, b, h)

    def reduce_block(d, par, h, b):
        hops = len(table[d, par])
        sign = 1 if d == RIGHT else -1
        dest = wrap(tp + sign * (hops - h + 1), n_tp)
        if h > 1:
            rs(d, b, h - 1, dest).wait_recv()
            mine = partial[dest, rows(b, slots), :].astype(f32)
            chain[d, b, h - 2] = (chain[d, b, h - 2].astype(f32) + mine).astype(bf16)
        rs(d, b, h, dest).start()

    def send_reduce(d, par, h, step):
        for b in blocks_back(chip_back(step, par)):
            reduce_block(d, par, h, b)

    def norm_pair(pair):
        for par in (EVEN, ODD):
            c = chip_in(pair, par)
            for d in (RIGHT, LEFT):
                hops = len(table[d, par])
                for b in blocks_in(c):
                    ag(d, b, hops, hops).wait_recv()
            total = jnp.zeros((chunk, 128), f32)
            for t in range(n_tp):
                for k in range(0, width, 128):
                    v = gathered[t, rows(c, chunk), k:k + 128].astype(f32)
                    total = total + v * v
            mean = jnp.sum(total, axis=1, keepdims=True) / model_width
            scale = lax.rsqrt(mean + NORM_EPS)
            for t in range(n_tp):
                v = gathered[t, rows(c, chunk), :].astype(f32)
                g = pre_gain[:, t * width:(t + 1) * width]
                normed[par * chunk:(par + 1) * chunk, t * width:(t + 1) * width] = (
                    v * scale * g).astype(bf16)

    gu_tile = 2 * ffw // 3 if (2 * ffw // 3) % 128 == 0 else 2 * ffw

    def gate_up_tile(n):
        at = slice(n * gu_tile, (n + 1) * gu_tile)
        gate_up[:, at] = jnp.dot(normed[...], w_gu[:, at], preferred_element_type=f32)

    def activate():
        g = gate_up[:, :ffw]
        u = gate_up[:, ffw:]
        hidden[...] = (g / (1.0 + jnp.exp(-g)) * u).astype(bf16)

    def down_tile(pair, t):
        res = jnp.dot(hidden[...], w_dn[:, t * width:(t + 1) * width],
                      preferred_element_type=f32).astype(bf16)
        partial[t, rows(chip_in(pair, EVEN), chunk), :] = res[:chunk]
        partial[t, rows(chip_in(pair, ODD), chunk), :] = res[chunk:]

    def mix_matrix(c):
        e = 2 * c
        picked = jnp.concatenate([chosen[pl.ds(e, 1), :], chosen[pl.ds(e + 1, 1), :]], axis=1)
        weight = jnp.concatenate([route[pl.ds(e, 1), :], route[pl.ds(e + 1, 1), :]], axis=1)
        for row in range(0, tok, 128):
            at = lax.broadcasted_iota(jnp.int32, (128, chunk), 0) + row
            w = jnp.where(at == picked, weight, 0.0)
            hi = w.astype(bf16)
            lo = (w - hi.astype(f32)).astype(bf16)
            mix[c, row:row + 128, :] = jnp.concatenate([hi, lo], axis=1)

    def give_back(b, to):
        return pltpu.make_async_remote_copy(
            src_ref=summed.at[rows(b, slots), :],
            dst_ref=returned.at[rows(to, slots), :],
            send_sem=ret_s.at[b], recv_sem=ret_r.at[to],
            device_id={"ep": b}, device_id_type=MESH)

    def finish_block(par, b):
        total = partial[tp, rows(b, slots), :].astype(f32)
        for d in (RIGHT, LEFT):
            hops = len(table[d, par])
            rs(d, b, hops, tp).wait_recv()
            total = total + chain[d, b, hops - 1].astype(f32)
        total = total.astype(bf16)

        @pl.when(b != ep)
        def _():
            summed[rows(b, slots), :] = total
            give_back(b, ep).start()

        @pl.when(b == ep)
        def _():
            returned[rows(b, slots), :] = total

    def wait_returned(c):
        for k in range(2):
            e = 2 * c + k

            @pl.when(e != ep)
            def _():
                give_back(e, e).wait_recv()

    def chip_mixed(c, row):
        part = returned[rows(c, chunk), :]
        return mixed[row:row + 128, :] + jnp.dot(
            mix[c, row:row + 128, :], jnp.concatenate([part, part], axis=0), preferred_element_type=f32)

    def combine(c):
        wait_returned(c)
        for row in range(0, tok, 128):
            mixed[row:row + 128, :] = chip_mixed(c, row)

    def senders(step):
        pair = lax.rem(step + 1, n_pair)
        return wrap(y - pair - 1, n_y), wrap(y + pair, n_y)

    def gather_sent(pair):
        for (d, par), offsets in table.items():
            for b in blocks_in(chip_in(pair, par)):
                for h in range(1, len(offsets) + 1):
                    ag(d, b, h, h - 1).wait_send()

    def reduce_sent(step):
        for (d, par), offsets in table.items():
            for b in blocks_back(chip_back(step, par)):
                for h in range(1, len(offsets) + 1):
                    rs(d, b, h, tp).wait_send()

    n_gu = 2 * ffw // gu_tile
    pieces = [("norm",)] + [("gu", n) for n in range(n_gu)] + [("act",)] + [("dn", t) for t in range(n_tp)]
    share = -(-len(pieces) // (period - 1))

    def run_piece(piece, pair):
        if piece[0] == "norm":
            norm_pair(pair)
        elif piece[0] == "gu":
            gate_up_tile(piece[1])
        elif piece[0] == "act":
            activate()
        else:
            down_tile(pair, piece[1])

    own, twin = blocks_in(y)
    for d in (RIGHT, LEFT):
        gather_block(d, own, 1)
    dispatch(twin, ep).start()
    for j in range(n_pair):
        for rel in ((j, -j - 1) if j else (-1,)):
            for k in range(2):
                dispatch(2 * wrap(y + rel, n_y) + k, ep).start()
    wait_dispatched(twin)
    for d in (RIGHT, LEFT):
        gather_block(d, twin, 1)
    first = [(par, h, d) for (d, par), offsets in table.items()
             for h, at in enumerate(offsets, 1) if at < period]
    for par, h, d in sorted(m for m in first if m[0] == EVEN and m[1] > 1):
        send_gather(d, par, h, 0)
    for par, pair in ((ODD, 0), (EVEN, 1)):
        for b in blocks_in(chip_in(pair, par)):
            wait_dispatched(b)
            for d in (LEFT, RIGHT):
                gather_block(d, b, 1)
    for par, h, d in sorted(m for m in first if m[0] == ODD and m[1] > 1):
        send_gather(d, par, h, 0)
    for row in range(0, tok, 128):
        mixed[row:row + 128, :] = tokens[row:row + 128, :].astype(f32)

    last = rs0 + n_pair

    def round_(i, carry):
        for at, group in ((1, late[:1]), (2, late[1:])):
            @pl.when(i == at)
            def _():
                for load in group:
                    load.wait()

        for k in range(period):
            for par, at in ((EVEN, 0), (ODD, min(table[RIGHT, ODD][0], table[LEFT, ODD][0]))):
                if at == k:
                    @pl.when((i < n_pair) & (i != (1 if par == EVEN else 0)))
                    def _():
                        for b in blocks_in(chip_in(i, par)):
                            wait_dispatched(b)
            for (d, par), offsets in table.items():
                for h, at in enumerate(offsets, 1):
                    if at % period != k:
                        continue
                    ii = i - at // period

                    @pl.when((ii >= 0) & (ii < n_pair) & (ii != (1 if (par, h) == (EVEN, 1) else -1)))
                    def _():
                        send_gather(d, par, h, ii)

                    @pl.when((ii >= rs0) & (ii < rs0 + n_pair))
                    def _():
                        send_reduce(d, par, h, ii - rs0)

            pair = i - 2
            if k < period - 1:
                @pl.when((pair >= 0) & (pair < n_pair))
                def _():
                    for piece in pieces[k * share:(k + 1) * share]:
                        run_piece(piece, pair)

                if k == 0:
                    @pl.when(i <= n_pair)
                    def _():
                        for par in (EVEN, ODD):
                            mix_matrix(chip_in(i - 1, par))
                if k == 1:
                    @pl.when(i >= last - n_pair)
                    def _():
                        gather_sent(i - (last - n_pair))
        done = i - rs0 - 1

        @pl.when((done >= 0) & (done < n_pair))
        def _():
            for par in (EVEN, ODD):
                for b in blocks_back(chip_back(done, par)):
                    finish_block(par, b)

        @pl.when((done >= 1) & (done < n_pair))
        def _():
            for c in senders(done - 1):
                combine(c)
            reduce_sent(done - 1)
        return carry

    lax.fori_loop(1, last, round_, 0)

    end = n_pair - 1
    tail = sorted((at, d, par, h) for (d, par), offsets in table.items()
                  for h, at in enumerate(offsets, 1) if at >= period)
    cut = max(at for at, d, par, h in tail if par == EVEN)
    for at, d, par, h in tail:
        if at <= cut:
            send_reduce(d, par, h, end)
    combine(senders(end - 1)[0])
    for k in range(2):
        for at, d, par, h in tail:
            if at > cut:
                reduce_block(d, par, h, blocks_back(chip_back(end, par))[k])
    for b in blocks_back(chip_back(end, EVEN)):
        finish_block(EVEN, b)
    combine(senders(end - 1)[1])
    for b in blocks_back(chip_back(end, ODD)):
        finish_block(ODD, b)
    far, near = senders(end)
    combine(far)
    wait_returned(near)

    parts = []
    for row in range(0, tok, 128):
        v = chip_mixed(near, row)
        mixed[row:row + 128, :] = v
        v = v * v
        part = v[:, :128]
        for k in range(128, width, 128):
            part = part + v[:, k:k + 128]
        parts.append(part)
    row_sum = lax.dot_general(jnp.ones((8, 128), f32), jnp.concatenate(parts, axis=0),
                              (((1,), (1,)), ((), ())),
                              precision=lax.Precision.HIGHEST, preferred_element_type=f32)
    squares[tp] = row_sum[0:1, :]

    def share_squares(peer, at):
        return pltpu.make_async_remote_copy(
            src_ref=squares.at[at], dst_ref=squares.at[at],
            send_sem=sq_s.at[peer], recv_sem=sq_r.at[at],
            device_id={"tp": peer}, device_id_type=MESH)

    for k in range(n_tp // 2, 0, -1):
        for peer in {k, n_tp - k}:
            share_squares(wrap(tp + peer, n_tp), tp).start()

    reduce_sent(end - 1)
    reduce_sent(end)

    def sent_block(k, carry):
        b = wrap(ep + k, n_ep)
        dispatch(b, ep).wait_send()
        give_back(b, ep).wait_send()
        return carry

    lax.fori_loop(1, n_ep, sent_block, 0)

    for k in range(1, n_tp):
        peer = wrap(tp + k, n_tp)
        share_squares(peer, peer).wait_recv()
    total = squares[0]
    for t in range(1, n_tp):
        total = total + squares[t]
    scale_row = lax.rsqrt(total / model_width + NORM_EPS)
    scale = jnp.transpose(jnp.broadcast_to(scale_row, (8, tok)))[:, 0:1]
    scale_out[...] = jnp.broadcast_to(scale, scale_out.shape)
    for k in range(1, n_tp):
        share_squares(wrap(tp + k, n_tp), tp).wait_send()


def close(mixed, scale, out_gain, out):
    for k in range(0, out.shape[1], 128):
        out[:, k:k + 128] = (mixed[:, k:k + 128] * scale[...] * out_gain[:, k:k + 128]).astype(out.dtype)


def solution(mesh):
    n_ep, n_tp = mesh.shape["ep"], mesh.shape["tp"]

    def shards(tokens, pre_gain, out_gain, chosen, route_weight, expert_gate, expert_up, expert_down):
        tok, width = tokens.shape
        slots = chosen.shape[2]
        ffw = expert_gate.shape[2]
        model_width = pre_gain.shape[0]
        cap = n_ep * slots
        chunk = 2 * slots
        n_y = n_ep // 2
        hops = n_tp // 2
        bf16, f32 = jnp.bfloat16, jnp.float32
        vmem = pl.BlockSpec(memory_space=pltpu.VMEM)
        hbm = pl.BlockSpec(memory_space=pltpu.HBM)
        dma = pltpu.SemaphoreType.DMA
        mixed, scale = pl.pallas_call(
            functools.partial(kernel, n_ep, n_tp),
            name="routed_ffn",
            out_shape=(jax.ShapeDtypeStruct((tok, width), f32), jax.ShapeDtypeStruct((tok, 128), f32)),
            in_specs=[hbm] * 7,
            out_specs=(vmem, vmem),
            scratch_shapes=[
                pltpu.VMEM((tok, width), bf16),
                pltpu.VMEM((1, model_width), f32),
                pltpu.VMEM((n_ep, slots), jnp.int32),
                pltpu.VMEM((n_ep, slots), f32),
                pltpu.VMEM((cap, tok), bf16),
                pltpu.VMEM((cap, width), bf16),
                pltpu.VMEM((n_tp, cap, width), bf16),
                pltpu.VMEM((2 * chunk, model_width), bf16),
                pltpu.VMEM((model_width, 2 * ffw), bf16),
                pltpu.VMEM((ffw, model_width), bf16),
                pltpu.VMEM((2 * chunk, 2 * ffw), f32),
                pltpu.VMEM((2 * chunk, ffw), bf16),
                pltpu.VMEM((n_tp, cap, width), bf16),
                pltpu.VMEM((2, n_ep, hops, slots, width), bf16),
                pltpu.VMEM((cap, width), bf16),
                pltpu.VMEM((cap, width), bf16),
                pltpu.VMEM((n_y, tok, 2 * chunk), bf16),
                pltpu.VMEM((n_tp, 1, tok), f32),
                dma((7,)),
                dma((n_ep,)), dma((n_ep,)),
                dma((2, n_ep, hops)), dma((2, n_ep, hops)),
                dma((2, n_ep, hops)), dma((2, n_ep, hops)),
                dma((n_ep,)), dma((n_ep,)),
                dma((n_tp,)), dma((n_tp,)),
            ],
            compiler_params=pltpu.CompilerParams(
                collective_id=0, has_side_effects=True, vmem_limit_bytes=52 * 2**20),
        )(*(pltpu.with_memory_space_constraint(v, pltpu.HBM) for v in (
            tokens, pre_gain.reshape(1, -1), chosen[0], route_weight[0],
            expert_gate[0], expert_up[0], expert_down[0])))
        return pl.pallas_call(
            close,
            name="closing_norm",
            out_shape=jax.ShapeDtypeStruct((tok, width), bf16),
            in_specs=[vmem] * 3,
            out_specs=vmem,
            compiler_params=pltpu.CompilerParams(vmem_limit_bytes=8 * 2**20),
        )(mixed, scale, out_gain.reshape(1, -1))

    return jax.shard_map(
        shards,
        mesh=mesh,
        in_specs=(
            P(("grp", "ep"), "tp"),
            P(),
            P("tp"),
            P(("grp", "ep"), None, None),
            P(("grp", "ep"), None, None),
            P("ep", None, "tp"),
            P("ep", None, "tp"),
            P("ep", "tp", None),
        ),
        out_specs=P(("grp", "ep"), "tp"),
        check_vma=False,
    )
```

time: 165 us -> 160 us (0.970)
  Pallas kernels: 163 us -> 160 us
  local copies, waits for them, and re-layouts: 1.77 us -> 0.01 us
    pallas_call x1, Pallas kernels: 163 us -> 159 us  [shards(): pl.pallas_call(functools.partial(kernel, n_ep, n_tp), name='routed_ffn',...]
    unnamed x1 -> x2, local copies, waits for them, and re-layouts: 1.77 us -> 0.01 us
where the time goes in v2:
time: 160 us
  Pallas kernels  160 us (100%)
    pallas_call x1, Pallas kernels, shards(): pl.pallas_call(functools.partial(kernel, n_ep, n_tp), name='routed_ffn',...  159 us

profile of v2, /device:TPU:513, one launch (start us, length us, event | category | flops | bytes accessed | tf_op | source)
XLA Modules:
  0.0 159.7 jit_solution(2733935322036775470)
XLA Ops:
  0.0 0.0 copy-start
  0.0 158.9 %routed_ffn.1 = (f32[384,512]{1,0:T(8,128)S(1)}, f32[384,128]{1,0:T(8,128)S(1)}) custom-call(bf16[384,512]{1,0:T(8,128)(2,1)} %tokens_in.1, f32[1,4096]{1,0:T(1,128)} %bitcast.11, s32[16,48]{1,0:T(8,128)} %bitcast.12, f32[16,48]{1,0:T(8,128)} %bitcast.13, bf16[4096,384]{1,0:T(8,128)(2,1)} %bitcast.8, bf16[4096,384]{1,0:T(8,128)(2,1)} %bitcast.9, ...), custom_call_target="tpu_custom_call" | custom-call | tf_op jit(solution)/shard_map/routed_ffn/pallas_call | solution.py:442
  158.9 0.0 copy-done
  158.9 0.9 closing_norm.1
Async XLA Ops:
  0.0 158.9 %copy-start = (f32[512]{0:T(512)S(1)}, f32[512]{0:T(512)}, u32[]{:S(2)}) copy-start(f32[512]{0:T(512)} %param.10) | copy-start | bytes 6148

commit v3 on v2

--- a/solution.py
+++ b/solution.py
@@ -221,15 +221,18 @@
             def _():
                 give_back(e, e).wait_recv()
 
-    def chip_mixed(c, row):
-        part = returned[rows(c, chunk), :]
-        return mixed[row:row + 128, :] + jnp.dot(
-            mix[c, row:row + 128, :], jnp.concatenate([part, part], axis=0), preferred_element_type=f32)
+    half = width // 2
+
+    def chip_mixed(c, n):
+        at = slice(n * half, (n + 1) * half)
+        part = returned[rows(c, chunk), at]
+        return mixed[:, at] + jnp.dot(
+            mix[c], jnp.concatenate([part, part], axis=0), preferred_element_type=f32)
 
     def combine(c):
         wait_returned(c)
-        for row in range(0, tok, 128):
-            mixed[row:row + 128, :] = chip_mixed(c, row)
+        for n in range(2):
+            mixed[:, n * half:(n + 1) * half] = chip_mixed(c, n)
 
     def senders(step):
         pair = lax.rem(step + 1, n_pair)
@@ -332,6 +335,13 @@
                     @pl.when(i >= last - n_pair)
                     def _():
                         gather_sent(i - (last - n_pair))
+                back = i - rs0 - 2
+                for at, work in ((period - 3, lambda: combine(senders(back)[0])), (period - 2, lambda: combine(senders(back)[1])),
+                                 (0, lambda: reduce_sent(back))):
+                    if k == at:
+                        @pl.when((back >= 0) & (back < n_pair))
+                        def _():
+                            work()
         done = i - rs0 - 1
 
         @pl.when((done >= 0) & (done < n_pair))
@@ -339,12 +349,6 @@
             for par in (EVEN, ODD):
                 for b in blocks_back(chip_back(done, par)):
                     finish_block(par, b)
-
-        @pl.when((done >= 1) & (done < n_pair))
-        def _():
-            for c in senders(done - 1):
-                combine(c)
-            reduce_sent(done - 1)
         return carry
 
     lax.fori_loop(1, last, round_, 0)
@@ -356,33 +360,29 @@
     for at, d, par, h in tail:
         if at <= cut:
             send_reduce(d, par, h, end)
-    combine(senders(end - 1)[0])
     for k in range(2):
         for at, d, par, h in tail:
             if at > cut:
                 reduce_block(d, par, h, blocks_back(chip_back(end, par))[k])
+    reduce_sent(end - 1)
     for b in blocks_back(chip_back(end, EVEN)):
         finish_block(EVEN, b)
-    combine(senders(end - 1)[1])
+    for c in senders(end - 1):
+        combine(c)
     for b in blocks_back(chip_back(end, ODD)):
         finish_block(ODD, b)
     far, near = senders(end)
     combine(far)
     wait_returned(near)
 
-    parts = []
-    for row in range(0, tok, 128):
-        v = chip_mixed(near, row)
-        mixed[row:row + 128, :] = v
-        v = v * v
-        part = v[:, :128]
-        for k in range(128, width, 128):
-            part = part + v[:, k:k + 128]
-        parts.append(part)
-    row_sum = lax.dot_general(jnp.ones((8, 128), f32), jnp.concatenate(parts, axis=0),
-                              (((1,), (1,)), ((), ())),
-                              precision=lax.Precision.HIGHEST, preferred_element_type=f32)
-    squares[tp] = row_sum[0:1, :]
+    part = jnp.zeros((tok, 128), f32)
+    for n in range(2):
+        v = chip_mixed(near, n)
+        mixed[:, n * half:(n + 1) * half] = v
+        for k in range(0, half, 128):
+            w = v[:, k:k + 128]
+            part = part + w * w
+    squares[tp] = jnp.sum(jnp.transpose(part), axis=0, keepdims=True)
 
     def share_squares(peer, at):
         return pltpu.make_async_remote_copy(
@@ -394,7 +394,6 @@
         for peer in {k, n_tp - k}:
             share_squares(wrap(tp + peer, n_tp), tp).start()
 
-    reduce_sent(end - 1)
     reduce_sent(end)
 
     def sent_block(k, carry):

time: 160 us -> 160 us (level)
  no operation moved by 1% of the time
where the time goes in v3:
time: 160 us
  Pallas kernels  160 us (100%)
    pallas_call x1, Pallas kernels, shards(): pl.pallas_call(functools.partial(kernel, n_ep, n_tp), name='routed_ffn',...  159 us

profile of v3, /device:TPU:513, one launch (start us, length us, event | category | flops | bytes accessed | tf_op | source)
XLA Modules:
  0.0 159.8 jit_solution(8897087851733793552)
XLA Ops:
  0.0 0.0 copy-start
  0.0 158.9 %routed_ffn.1 = (f32[384,512]{1,0:T(8,128)S(1)}, f32[384,128]{1,0:T(8,128)S(1)}) custom-call(bf16[384,512]{1,0:T(8,128)(2,1)} %tokens_in.1, f32[1,4096]{1,0:T(1,128)} %bitcast.11, s32[16,48]{1,0:T(8,128)} %bitcast.12, f32[16,48]{1,0:T(8,128)} %bitcast.13, bf16[4096,384]{1,0:T(8,128)(2,1)} %bitcast.8, bf16[4096,384]{1,0:T(8,128)(2,1)} %bitcast.9, ...), custom_call_target="tpu_custom_call" | custom-call | tf_op jit(solution)/shard_map/routed_ffn/pallas_call | solution.py:441
  158.9 0.0 copy-done
  158.9 0.9 closing_norm.1
Async XLA Ops:
  0.0 158.9 %copy-start = (f32[512]{0:T(512)S(1)}, f32[512]{0:T(512)}, u32[]{:S(2)}) copy-start(f32[512]{0:T(512)} %param.10) | copy-start | bytes 6148
